TPU v7x, 512 devices: a whole 4x8x8 slice. The times are simulated.
512 devices in a mesh: ep: 32 (over z, x), tp: 16 (over y, core).
Axes of the slice: x: 4, y: 8, z: 8, core: 2. Of those that a mesh axis runs over, the one named last changes fastest.
Arguments:
- query_latent: bfloat16 [8192, 768], P('ep'), may hold values from -600 to 600
- shared_latent: bfloat16 [8192, 512], P('ep'), may hold values from -600 to 600
- rotary_key: bfloat16 [8192, 64], P('ep'), may hold values from -2500 to 2500
- query_gain: float32 [768], replicated, may hold values from 0.1 to 1.9
- shared_gain: float32 [512], replicated, may hold values from 0.1 to 1.9
- query_plain_weight: bfloat16 [768, 2048], P(None, 'tp'), may hold values from -0.21875 to 0.21875
- query_turn_weight: bfloat16 [768, 1024], P(None, 'tp'), may hold values from -0.21875 to 0.21875
- key_weight: bfloat16 [512, 2048], P(None, 'tp'), may hold values from -0.25 to 0.25
- value_weight: bfloat16 [512, 2048], P(None, 'tp'), may hold values from -0.25 to 0.25
- mixer_out_weight: bfloat16 [2048, 2048], P('tp'), may hold values from -1 to 1
- expert_input: bfloat16 [4096, 2048], P('ep'), may hold values from -600 to 600
- expert_gain: float32 [2048], replicated, may hold values from 0.1 to 1.9
- routing: int32 [4096, 4], P('ep'), may hold values from 0 to 31, all different within a row; in each aligned block of 128 rows (0 to 127, 128 to 255, ...) at most 21 rows name the same one
- routing_weight: float32 [4096, 4], P('ep'), may hold values from 0.05 to 1
- gate_weight: bfloat16 [32, 2048, 2048], P('ep', None, 'tp'), may hold values from -0.375 to 0.375
- up_weight: bfloat16 [32, 2048, 2048], P('ep', None, 'tp'), may hold values from -0.375 to 0.375
- down_weight: bfloat16 [32, 2048, 2048], P('ep', 'tp'), may hold values from -0.01953125 to 0.01953125
Outputs:
- mixer_output: bfloat16 [8192, 2048], P('ep')
- expert_output: bfloat16 [4096, 2048], P('ep')
Inputs may be any that keep to these rules, and one draw needn't show every extreme that they name: `routing`: each row names 4 different experts. In each aligned block of 128 rows (the rows of one index of ep) no expert is named by more than 21 rows, and in some block some expert is named by exactly 21.
All inputs are finite; a program needn't handle non-finite values.
Results may differ from a plain program's by a relative error of at most 0.019.
Values may be sent and summed in bfloat16 or wider, within the bound.
A program may use at most 128 MiB of HBM per device.

v0:
```python
import jax
import jax.numpy as jnp
from jax import lax
from jax.sharding import Mesh
from jax.sharding import PartitionSpec as P

NOPE = 128
ROPE = 64
VDIM = 128
TP = ("tp_0", "tp_1")
EPSILON = 1e-06
CLAMP_LIMIT = 7.0
SLOPE = 1.702
ROTARY_BASE = 10000.0
NEGATIVE = -1e30


def sent_together(arrays, axis, dim, along):
    columns = [a.reshape(*a.shape[:along], -1) for a in arrays]
    both = jnp.concatenate(columns, axis=along)
    out, at, done = (lax.all_gather(both, axis, axis=dim, tiled=True), 0, [])
    for a, column in zip(arrays, columns):
        share = out[..., at : at + column.shape[along]]
        done.append(share.reshape(*share.shape[:along], *a.shape[along:]))
        at += column.shape[along]
    return tuple(done)


def padded_to(lines, length):
    spare = -len(lines) % length
    return jnp.pad(lines, [(0, spare)] + [(0, 0)] * (lines.ndim - 1))


def sum_in_order(pieces, axes, turns):
    inside = pieces.shape[1:]
    pieces = pieces.reshape(*(lax.axis_size(a) for a in axes), *inside)
    pieces = jnp.moveaxis(pieces, turns, range(len(axes))).reshape(-1, *inside)
    for k in turns:
        pieces = lax.psum_scatter(pieces, axes[k], scatter_dimension=0, tiled=True)
    return pieces[0]


def gather_in_order(shard, axes, turns):
    pieces = shard[None]
    for k in turns:
        pieces = lax.all_gather(pieces, axes[k], axis=0, tiled=True)
    block = [lax.axis_size(axes[k]) for k in reversed(turns)]
    pieces = pieces.reshape(*block, *shard.shape)
    turned = sorted(range(len(turns)), key=lambda place: turns[len(turns) - 1 - place])
    return pieces.transpose(*turned, *range(len(turns), pieces.ndim)).reshape(-1, *shard.shape)


def sum_by_parts(shard, axes, turns):
    length, lines = (lax.axis_size(axes), shard.reshape(-1, *shard.shape[1:][-1:]))
    pieces = padded_to(lines, length).reshape(length, -1, *lines.shape[1:])
    own = sum_in_order(pieces, axes, turns)
    whole = gather_in_order(own, axes, turns[::-1]).reshape(-1, *lines.shape[1:])
    return whole[: len(lines)].reshape(shard.shape)


def sum_by_parts_2(shard, axis):
    lines = shard.reshape(-1, *shard.shape[1:][-1:])
    padded = padded_to(lines, lax.axis_size(axis))
    own = lax.psum_scatter(padded, axis, scatter_dimension=0, tiled=True)
    whole = lax.all_gather(own, axis, axis=0, tiled=True)
    return whole[: len(lines)].reshape(shard.shape)


def norm_rows(values, gains):
    widened = values.astype(jnp.float32)
    normed = widened * lax.rsqrt(jnp.mean(widened * widened, axis=-1, keepdims=True) + EPSILON)
    return (normed * gains).astype(jnp.bfloat16)


def rotary(values, position):
    half_dim = values.shape[-1] // 2
    frequency = ROTARY_BASE ** (-2.0 * jnp.arange(half_dim, dtype=jnp.float32) / values.shape[-1])
    angles = position.astype(jnp.float32)[:, None, None] * frequency[None, None, :]
    cosine = jnp.cos(angles)
    sine_part = jnp.sin(angles)
    lower = values[..., :half_dim]
    upper = values[..., half_dim:]
    return jnp.concatenate(
        [lower * cosine - upper * sine_part, upper * cosine + lower * sine_part], axis=-1
    )


def mixer_part(
    query_latent,
    shared_latent,
    rotary_key,
    query_gain,
    shared_gain,
    query_plain_weight,
    query_turn_weight,
    key_weight,
    value_weight,
    mixer_out_weight,
):
    row_count = query_latent.shape[0]
    head_count = query_plain_weight.shape[1] // NOPE
    position = lax.axis_index("ep") * row_count + jnp.arange(row_count, dtype=jnp.int32)
    query_normed = norm_rows(query_latent, query_gain)
    shared_normed = norm_rows(shared_latent, shared_gain)
    query_plain = jnp.dot(query_normed, query_plain_weight, preferred_element_type=jnp.float32)
    query_plain = query_plain.astype(jnp.bfloat16).reshape(row_count, head_count, NOPE)
    query_raw = jnp.dot(query_normed, query_turn_weight, preferred_element_type=jnp.float32)
    query_turned = rotary(query_raw.reshape(row_count, head_count, ROPE), position).astype(
        jnp.bfloat16
    )
    key_turned = rotary(rotary_key.astype(jnp.float32).reshape(row_count, 1, ROPE), position)
    key_turned = key_turned.astype(jnp.bfloat16).reshape(row_count, ROPE)
    scaling = (NOPE + ROPE) ** (-0.5)
    own_keys = jnp.dot(shared_normed, key_weight, preferred_element_type=jnp.float32)
    own_keys = own_keys.astype(jnp.bfloat16).reshape(row_count, head_count, NOPE)
    own_values = jnp.dot(shared_normed, value_weight, preferred_element_type=jnp.float32)
    own_values = own_values.astype(jnp.bfloat16).reshape(row_count, head_count, VDIM)
    portion = sent_together((own_keys, own_values, key_turned), "ep", 0, 1)
    key_plain = portion[0]
    key_total = key_plain.shape[0]
    peak_old = jnp.full((head_count, row_count), NEGATIVE, jnp.float32)
    scores = jnp.einsum("qhd,khd->hqk", query_plain, key_plain, preferred_element_type=jnp.float32)
    scores = scores + jnp.einsum(
        "qhr,kr->hqk", query_turned, portion[2], preferred_element_type=jnp.float32
    )
    scores = scores * scaling
    key_position = jnp.arange(key_total, dtype=jnp.int32)
    visible = (key_position[None, :] <= position[:, None])[None]
    scores = jnp.where(visible, scores, NEGATIVE)
    peak_new = jnp.maximum(peak_old, jnp.max(scores, axis=-1))
    weight = jnp.where(visible, jnp.exp(scores - peak_new[..., None]), 0.0)
    totals_new = jnp.sum(weight, axis=-1)
    accum_new = jnp.einsum(
        "hqk,khd->hqd", weight.astype(jnp.bfloat16), portion[1], preferred_element_type=jnp.float32
    )
    folded = (peak_new, totals_new, accum_new)
    peak_final, totals_final, accum_final = folded
    heads_out = accum_final / totals_final[..., None]
    heads_out = (
        jnp.transpose(heads_out, (1, 0, 2))
        .reshape(row_count, head_count * VDIM)
        .astype(jnp.bfloat16)
    )
    partial_value = jnp.dot(heads_out, mixer_out_weight, preferred_element_type=jnp.float32)
    return (
        sum_by_parts(partial_value.astype(jnp.bfloat16), TP, (0, 1))
        .astype(jnp.float32)
        .astype(jnp.bfloat16)
    )


def expert_part(
    expert_input, expert_gain, routing, routing_weight, gate_weight, up_weight, down_weight
):
    token_count = expert_input.shape[0]
    top_count = routing.shape[1]
    width = expert_input.shape[1]
    experts = lax.axis_size("ep")
    capacity = 4 * token_count * top_count // (3 * experts)
    normed = norm_rows(expert_input, expert_gain)
    flattened = routing.reshape(token_count * top_count)
    matches = (flattened[:, None] == jnp.arange(experts, dtype=jnp.int32)[None, :]).astype(
        jnp.int32
    )
    ranking = jnp.cumsum(matches, axis=0) - 1
    slot_index = jnp.sum(ranking * matches, axis=1)
    target = (flattened * capacity + slot_index).reshape(token_count, top_count)
    slot_ids = jnp.arange(experts * capacity, dtype=jnp.int32)
    select = target[None, :, :] == slot_ids[:, None, None]
    gather_table = jnp.any(select, axis=2).astype(jnp.bfloat16)
    outgoing = jnp.dot(gather_table, normed, preferred_element_type=jnp.float32).astype(
        jnp.bfloat16
    )
    outgoing = outgoing.reshape(experts, capacity, width)
    arrived = lax.all_to_all(outgoing, "ep", split_axis=0, concat_axis=0, tiled=True).reshape(
        experts * capacity, width
    )
    gate_local = gate_weight[0]
    up_local = up_weight[0]
    down_local = down_weight[0]
    gate_pre = jnp.minimum(
        jnp.dot(arrived, gate_local, preferred_element_type=jnp.float32), CLAMP_LIMIT
    )
    up_pre = jnp.clip(
        jnp.dot(arrived, up_local, preferred_element_type=jnp.float32), -CLAMP_LIMIT, CLAMP_LIMIT
    )
    hidden = ((up_pre + 1.0) * (gate_pre * jax.nn.sigmoid(SLOPE * gate_pre))).astype(jnp.bfloat16)
    partial_value = jnp.dot(hidden, down_local, preferred_element_type=jnp.float32)
    summed = sum_by_parts_2(partial_value.astype(jnp.bfloat16), TP).astype(jnp.float32)
    summed = summed.astype(jnp.bfloat16).reshape(experts, capacity, width)
    returned_rows = lax.all_to_all(summed, "ep", split_axis=0, concat_axis=0, tiled=True).reshape(
        experts * capacity, width
    )
    mixing = jnp.transpose(jnp.sum(jnp.where(select, routing_weight[None, :, :], 0.0), axis=2))
    result = jnp.dot(mixing, returned_rows.astype(jnp.float32))
    return result.astype(jnp.bfloat16)


def per_device(
    query_latent,
    shared_latent,
    rotary_key,
    query_gain,
    shared_gain,
    query_plain_weight,
    query_turn_weight,
    key_weight,
    value_weight,
    mixer_out_weight,
    expert_input,
    expert_gain,
    routing,
    routing_weight,
    gate_weight,
    up_weight,
    down_weight,
):
    mixer_output = mixer_part(
        query_latent,
        shared_latent,
        rotary_key,
        query_gain,
        shared_gain,
        query_plain_weight,
        query_turn_weight,
        key_weight,
        value_weight,
        mixer_out_weight,
    )
    expert_output = expert_part(
        expert_input, expert_gain, routing, routing_weight, gate_weight, up_weight, down_weight
    )
    return (mixer_output, expert_output)


def solution(mesh):
    finer = Mesh(mesh.devices.reshape(mesh.shape["ep"], 8, 2), ("ep", "tp_0", "tp_1"))
    placed = (
        P("ep", None),
        P("ep", None),
        P("ep", None),
        P(),
        P(),
        P(None, TP),
        P(None, TP),
        P(None, TP),
        P(None, TP),
        P(TP, None),
        P("ep", None),
        P(),
        P("ep", None),
        P("ep", None),
        P("ep", None, TP),
        P("ep", None, TP),
        P("ep", TP, None),
    )
    return jax.shard_map(
        per_device,
        mesh=finer,
        in_specs=placed,
        out_specs=(P("ep", None), P("ep", None)),
        check_vma=False,
    )
```

profile of v0, /device:TPU:2, one launch (start us, length us, event | category | flops | bytes accessed | tf_op | source)
XLA Modules:
  0.0 364.6 jit_solution(4953756799054424215)
XLA Ops:
  7.2 0.0 copy-start
  7.2 0.0 copy-start.1
  7.2 0.0 all-gather.5.cloned.1.call-start
  7.3 1.2 fusion.33
  8.5 0.8 bitcast_convert_fusion
  9.3 1.1 fusion.36
  10.4 1.3 convolution_convert_fusion.4
  11.7 1.3 convolution_convert_fusion.5
  13.0 1.3 convolution_bitcast_fusion.2
  14.3 0.3 fusion.85
  14.6 0.7 pad_maximum_fusion
  15.2 0.0 all-gather.5.cloned.1.call-update
  15.3 0.0 all-gather.9.cloned.1.call-start
  15.3 0.8 copy.44
  16.1 0.1 eq.42
  16.2 0.1 eq.38
  16.3 1.2 reduce-window.6
  17.5 0.2 slice_reduce_fusion
  17.8 0.1 fusion.62
  17.9 0.1 reduce_sum.60
  18.0 0.1 copy.47
  18.1 0.7 multiply_add_fusion
  18.8 0.2 fusion.29
  19.0 0.2 fusion.11
  19.1 2.0 convolution_convert_fusion.1
  21.1 2.5 reshape.278
  23.7 97.5 %all_to_all.10 = bf16[32,21,2048]{2,1,0:T(8,128)(2,1)} all-to-all(bf16[32,21,2048]{2,1,0:T(8,128)(2,1)} %reshape.278), channel_id=1, replica_groups=mesh['ep'=32,'tp_0'=8,'tp_1'=2] {'ep'}, dimensions={0} | all-to-all | bytes 5505024 | tf_op jit(solution)/shard_map/all_to_all | solution.py:175
  121.1 3.1 reshape.279
  124.2 2.6 convolution_minimum_fusion
  126.8 5.7 %convolution_convert_fusion = bf16[672,2048]{1,0:T(8,128)(2,1)} fusion(bf16[672,2048]{1,0:T(8,128)(2,1)S(1)} %reshape.279, bf16[1,128,2048]{2,1,0:T(8,128)(2,1)S(1)} %copy-done, bf16[1,2048,128]{2,1,0:T(8,128)(2,1)} %param.32, f32[672,128]{1,0:T(8,128)} %convolution_minimum_fusion), kind=kOutput, calls=%fused_computation.11 | convolution fusion | flops 706793472 | bytes 6897664 | tf_op jit(solution)/shard_map/dot_general | solution.py:188
  132.5 35.4 %fusion = bf16[48,2048]{1,0:T(8,128)(2,1)S(1)} fusion(bf16[672,2048]{1,0:T(8,128)(2,1)} %convolution_convert_fusion), kind=kCustom, calls=%all-reduce-scatter | all-reduce-scatter fusion | flops 1572865 | bytes 2951168
  167.9 1.3 collective-permute-start
  169.3 1.3 collective-permute-start.1
  170.6 1.3 dynamic-slice.4
  172.5 2.1 collective-permute-done.1
  174.6 0.0 collective-permute-done
  174.6 0.8 concatenate.30
  175.4 0.7 dynamic-slice_bitcast_fusion
  176.1 0.0 all-gather.9.cloned.1.call-update
  176.2 0.0 all-gather.5.cloned.1.call-done
  176.2 6.3 %convolution_bitcast_fusion.1 = f32[1,256,8192]{2,1,0:T(8,128)} fusion(bf16[8192,320]{0,1:T(8,128)(2,1)} %all-gather.5.cloned.1.call-done, bf16[768,128]{1,0:T(8,128)(2,1)S(1)} %copy-done.3, bf16[256,768]{1,0:T(8,128)(2,1)S(1)} %copy-done.2, f32[768]{0:T(1024)S(1)} %copy-done.5, f32[256]{0:T(256)S(1)} %add_rsqrt_fusion.1), kind=kOutput, calls=%fused_computation.1 | convolution fusion | flops 588021760 | bytes 11079680 | tf_op jit(solution)/shard_map/qhd,khd->hqk/dot_general | solution.py:122
  182.5 6.9 %fusion.96 = (f32[256]{0:T(256)S(1)}, f32[1,256,8192]{2,1,0:T(8,128)}) fusion(f32[1,256,8192]{2,1,0:T(8,128)} %convolution_bitcast_fusion.1, bf16[256,32]{0,1:T(8,128)(2,1)S(1)} %get-tuple-element.3, bf16[256,32]{0,1:T(8,128)(2,1)S(1)} %get-tuple-element.2, bf16[8192,320]{0,1:T(8,128)(2,1)} %all-gather.5.cloned.1.call-done, s32[256]{0:T(256)S(1)} %iota_add_fusion), kind=kOutput, calls=%fused_computation.113 | convolution fusion | flops 278986496 | bytes 17860608 | tf_op jit(solution)/shard_map/qhr,kr->hqk/dot_general | solution.py:123
  189.4 30.8 %all-gather.9.cloned.1.call-done = bf16[16,42,2048]{2,1,0:T(8,128)(2,1)} async-done(((bf16[1,42,2048]{2,1,0:T(8,128)(2,1)}), bf16[16,42,2048]{2,1,0:T(8,128)(2,1)}) %all-gather.9.cloned.1.call-update) | async-done | bytes 2752528 | tf_op jit(solution)/shard_map/all_gather | solution.py:65
  220.2 5.3 %reshape.280 = bf16[32,21,2048]{2,1,0:T(8,128)(2,1)} reshape(bf16[16,42,2048]{2,1,0:T(8,128)(2,1)} %all-gather.9.cloned.1.call-done) | data formatting | bytes 5505024 | tf_op jit(solution)/shard_map/reshape | solution.py:190
  225.6 10.6 %all-to-all-start.1 = ((bf16[32,21,2048]{2,1,0:T(8,128)(2,1)}), bf16[32,21,2048]{2,1,0:T(8,128)(2,1)}, u32[]{:S(2)}, u32[]{:S(2)}) async-start(bf16[32,21,2048]{2,1,0:T(8,128)(2,1)} %reshape.280), calls=%async_computation.3 | async-start | bytes 6291456 | tf_op jit(solution)/shard_map/all_to_all | solution.py:191
  236.1 0.2 reduce-scatter.5.cloned.1.call-start
  236.3 0.0 copy-start.7
  236.4 4.7 %fusion.4 = f32[256]{0:T(256)S(1)} fusion(f32[1,256,8192]{2,1,0:T(8,128)} %get-tuple-element.9, f32[256]{0:T(256)S(1)} %broadcast_maximum_fusion, s32[256]{0:T(256)S(1)} %iota_add_fusion), kind=kLoop, calls=%fused_computation.7 | loop fusion | flops 8388352 | bytes 8391680 | tf_op jit(solution)/shard_map/reduce_sum | solution.py:132
  241.0 0.0 copy-start.6
  241.0 7.5 %convolution_convert_fusion.2 = bf16[256,2048]{1,0:T(8,128)(2,1)} fusion(bf16[128,2048]{1,0:T(8,128)(2,1)S(1)} %copy-done.7, bf16[8192,320]{0,1:T(8,128)(2,1)} %all-gather.5.cloned.1.call-done, f32[1,256,8192]{2,1,0:T(8,128)} %get-tuple-element.9, f32[256]{0:T(256)S(1)} %broadcast_maximum_fusion, s32[256]{0:T(256)S(1)} %iota_add_fusion, f32[256]{0:T(256)S(1)} %fusion.4), kind=kOutput, calls=%fused_computation.13 | convolution fusion | flops 680067072 | bytes 12061696 | tf_op jit(solution)/shard_map/dot_general | solution.py:144
  248.5 0.0 reduce-scatter.5.cloned.1.call-update
  248.5 0.0 reduce-scatter.7.cloned.1.call-start
  248.6 39.5 %reduce-scatter.5.cloned.1.call-done = bf16[2,16,2048]{2,1,0:T(8,128)(2,1)} async-done(((bf16[16,16,2048]{2,1,0:T(8,128)(2,1)}), bf16[2,16,2048]{2,1,0:T(8,128)(2,1)}) %reduce-scatter.5.cloned.1.call-update) | async-done | bytes 131088 | tf_op jit(solution)/shard_map/reduce_scatter | solution.py:39
  288.1 0.0 reduce-scatter.7.cloned.1.call-update
  288.1 0.0 all-gather.7.cloned.1.call-start
  288.2 17.4 %reduce-scatter.7.cloned.1.call-done = bf16[1,16,2048]{2,1,0:T(8,128)(2,1)} async-done(((bf16[2,16,2048]{2,1,0:T(8,128)(2,1)}), bf16[1,16,2048]{2,1,0:T(8,128)(2,1)}) %reduce-scatter.7.cloned.1.call-update) | async-done | bytes 65552 | tf_op jit(solution)/shard_map/reduce_scatter | solution.py:39
  305.5 3.5 all_gather.13
  309.1 0.0 all-gather.7.cloned.1.call-update
  309.1 0.1 select_reduce_fusion
  309.3 42.1 %all-gather.7.cloned.1.call-done = bf16[16,16,2048]{2,1,0:T(8,128)(2,1)} async-done(((bf16[2,16,2048]{2,1,0:T(8,128)(2,1)}), bf16[16,16,2048]{2,1,0:T(8,128)(2,1)}) %all-gather.7.cloned.1.call-update) | async-done | bytes 1048592 | tf_op jit(solution)/shard_map/all_gather | solution.py:46
  351.3 0.0 all-to-all-done.1
  351.3 3.0 reshape.281
  354.4 1.4 fusion.97
  355.8 2.3 copy.52
  (23 shorter events, 0.2 us)
Async XLA Ops:
  7.2 119.7 %copy-start = (bf16[1,128,2048]{2,1,0:T(8,128)(2,1)S(1)}, bf16[1,128,2048]{2,1,0:T(8,128)(2,1)}, u32[]{:S(2)}) copy-start(bf16[1,128,2048]{2,1,0:T(8,128)(2,1)} %param.33) | copy-start | bytes 1572868
  7.2 11.6 %copy-start.1 = (bf16[128,2048]{1,0:T(8,128)(2,1)S(1)}, bf16[128,2048]{1,0:T(8,128)(2,1)}, u32[]{:S(2)}) copy-start(bf16[128,2048]{1,0:T(8,128)(2,1)} %param.27) | copy-start | bytes 1572868
  7.2 11.9 %copy-start.4 = (f32[2048]{0:T(1024)S(1)}, f32[2048]{0:T(1024)}, u32[]{:S(2)}) copy-start(f32[2048]{0:T(1024)} %param.28) | copy-start | bytes 24580
  7.2 169.0 %all-gather.5.cloned.1.call-start = ((), (), s32[]{:S(2)}) async-start(), calls=%async_computation.4 | async-start | bytes 5406720 | tf_op jit(solution)/shard_map/all_gather | solution.py:21
  15.3 204.9 %all-gather.9.cloned.1.call-start = ((), (), s32[]{:S(2)}) async-start(), calls=%async_computation.8 | async-start | bytes 3342336 | tf_op jit(solution)/shard_map/all_gather | solution.py:65
  132.5 43.7 %copy-start.2 = (bf16[256,768]{1,0:T(8,128)(2,1)S(1)}, bf16[256,768]{1,0:T(8,128)(2,1)}, u32[]{:S(2)}) copy-start(bf16[256,768]{1,0:T(8,128)(2,1)} %param.17) | copy-start | bytes 1179652
  132.5 43.7 %copy-start.3 = (bf16[768,128]{1,0:T(8,128)(2,1)S(1)}, bf16[768,128]{1,0:T(8,128)(2,1)}, u32[]{:S(2)}) copy-start(bf16[768,128]{1,0:T(8,128)(2,1)} %param.22) | copy-start | bytes 589828
  132.5 43.7 %copy-start.5 = (f32[768]{0:T(1024)S(1)}, f32[768]{0:T(1024)}, u32[]{:S(2)}) copy-start(f32[768]{0:T(1024)} %param.20) | copy-start | bytes 9220
  167.9 6.7 %collective-permute-start = (bf16[48,2048]{1,0:T(8,128)(2,1)S(1)}, bf16[48,2048]{1,0:T(8,128)(2,1)S(1)}, u32[]{:S(2)}, u32[]{:S(2)}) collective-permute-start(bf16[48,2048]{1,0:T(8,128)(2,1)S(1)} %fusion), channel_id=1, source_target_pairs={{0,1},{1,2},{2,3},{3,4},{4,5},{5,6},{6,7},{7,8},{8,9},{9,10},{10,1... | collective-permute-start | bytes 589832
  169.3 5.3 %collective-permute-start.1 = (bf16[42,2048]{1,0:T(8,128)(2,1)S(1)}, bf16[42,2048]{1,0:T(8,128)(2,1)S(1)}, u32[]{:S(2)}, u32[]{:S(2)}) collective-permute-start(bf16[42,2048]{1,0:T(8,128)(2,1)S(1)} %slice.44), channel_id=1, source_target_pairs={{0,2},{1,3},{2,4},{3,5},{4,6},{5,7},{6,8},{7,9},{8,10},{9,11},{10,... | collective-permute-start | bytes 516104
  225.6 125.8 %all-to-all-start.1 = ((bf16[32,21,2048]{2,1,0:T(8,128)(2,1)}), bf16[32,21,2048]{2,1,0:T(8,128)(2,1)}, u32[]{:S(2)}, u32[]{:S(2)}) async-start(bf16[32,21,2048]{2,1,0:T(8,128)(2,1)} %reshape.280), calls=%async_computation.3 | async-start | bytes 6291456 | tf_op jit(solution)/shard_map/all_to_all | solution.py:191
  236.1 52.0 %reduce-scatter.5.cloned.1.call-start = ((), (), s32[]{:S(2)}) async-start(), calls=%async_computation.5 | async-start | bytes 1179648 | tf_op jit(solution)/shard_map/reduce_scatter | solution.py:39
  236.3 4.7 %copy-start.7 = (bf16[128,2048]{1,0:T(8,128)(2,1)S(1)}, bf16[128,2048]{1,0:T(8,128)(2,1)}, u32[]{:S(2)}) copy-start(bf16[128,2048]{1,0:T(8,128)(2,1)} %param.26) | copy-start | bytes 1572868
  241.0 68.1 %copy-start.6 = (f32[128,4]{0,1:T(4,128)S(1)}, f32[128,4]{0,1:T(4,128)}, u32[]{:S(2)}) copy-start(f32[128,4]{0,1:T(4,128)} %param.30) | copy-start | bytes 6148
  248.5 57.0 %reduce-scatter.7.cloned.1.call-start = ((), (), s32[]{:S(2)}) async-start(), calls=%async_computation.6 | async-start | bytes 196608 | tf_op jit(solution)/shard_map/reduce_scatter | solution.py:39
  288.1 63.2 %all-gather.7.cloned.1.call-start = ((), (), s32[]{:S(2)}) async-start(), calls=%async_computation.7 | async-start | bytes 1179648 | tf_op jit(solution)/shard_map/all_gather | solution.py:46
Sparse Core Ops, SparseCore 0:
  15.4 132.1 all-gather.4
  176.3 43.9 all-gather.8
  248.6 39.4 reduce-scatter.4
  290.7 14.8 reduce-scatter.6
  309.2 42.0 all-gather.6
where the time goes:
time: 366 us; the launch traced here: 365 us
  blocking collectives  136 us (37%)
  waiting for transfers between devices  132 us (36%)
  matrix products  36.3 us (10%)
  local copies, waits for them, and re-layouts  20.5 us (6%)
  between operations  14.7 us (4%)
  starting transfers between devices  13.5 us (4%)
  other arithmetic  11.2 us (3%)
    all_to_all x1, blocking collectives, expert_part(): lax.all_to_all(outgoing, 'ep', split_axis=0, concat_axis=0, tiled=True)  97.5 us
    reduce_scatter x2, waiting for transfers between devices, sum_in_order(): pieces = lax.psum_scatter(pieces, axes[k], scatter_dimension=0, tiled=True)  56.9 us
    all_gather x1, waiting for transfers between devices, gather_in_order(): pieces = lax.all_gather(pieces, axes[k], axis=0, tiled=True)  42.1 us
    unnamed x1, blocking collectives  35.4 us
    all_gather x1, waiting for transfers between devices, sum_by_parts_2(): whole = lax.all_gather(own, axis, axis=0, tiled=True)  30.8 us
    all_to_all x1, starting transfers between devices, expert_part(): lax.all_to_all(summed, 'ep', split_axis=0, concat_axis=0, tiled=True)  10.6 us
    dot_general x1, matrix products, mixer_part(): jnp.dot(heads_out, mixer_out_weight, preferred_element_type=jnp.float32)  7.46 us
  transfers between devices with their start and end apart: 8, of which 5 were waited for; matrix products, arithmetic and copies ran while one was open for 23% of the time, Pallas kernels for 0%

commit v1 on v0

--- a/solution.py
+++ b/solution.py
@@ -62,7 +62,16 @@
     lines = shard.reshape(-1, *shard.shape[1:][-1:])
     padded = padded_to(lines, lax.axis_size(axis))
     own = lax.psum_scatter(padded, axis, scatter_dimension=0, tiled=True)
-    whole = lax.all_gather(own, axis, axis=0, tiled=True)
+    wrap_rates = lambda m, across, d_out: jnp.concatenate(
+        jax.lax.all_to_all(
+            jnp.stack(jax.lax.axis_size(across) * [m], axis=0),
+            axis_name=across,
+            split_axis=0,
+            concat_axis=0,
+        ),
+        axis=d_out,
+    )
+    whole = wrap_rates(own, axis, 0)
     return whole[: len(lines)].reshape(shard.shape)
 
 

time: 366 us -> 390 us (1.066)
  waiting for transfers between devices: 132 us -> 235 us
  blocking collectives: 136 us -> 39.7 us
  starting transfers between devices: 13.5 us -> 34.6 us
    all_to_all x0 -> x2, waiting for transfers between devices: none -> 133 us  [the longest x1 74.9 us: expert_part(): lax.all_to_all(outgoing, 'ep', split_axis=0, concat_axis=0, tiled=True)]
    all_to_all x1 -> x0, blocking collectives: 97.5 us -> none  [expert_part(): lax.all_to_all(outgoing, 'ep', split_axis=0, concat_axis=0, tiled=True)]
    all_gather x1 -> x0, waiting for transfers between devices: 30.8 us -> none  [sum_by_parts_2(): whole = lax.all_gather(own, axis, axis=0, tiled=True)]
    all_to_all x0 -> x2, starting transfers between devices: none -> 23.6 us  [the longest x1 13.7 us: expert_part(): lax.all_to_all(outgoing, 'ep', split_axis=0, concat_axis=0, tiled=True)]
  transfers between devices with their start and end apart: 8 -> 9, of which waited for: 5 -> 6; matrix products, arithmetic and copies ran while one was open for 23% -> 20% of each run, Pallas kernels for 0% -> 0%
where the time goes in v1:
time: 390 us; the launch traced here: 389 us
  waiting for transfers between devices  235 us (60%)
  blocking collectives  39.7 us (10%)
  starting transfers between devices  34.6 us (9%)
  matrix products  33.3 us (9%)
  local copies, waits for them, and re-layouts  22 us (6%)
  between operations  14.8 us (4%)
  other arithmetic  9.49 us (2%)
    all_to_all x1, waiting for transfers between devices, expert_part(): lax.all_to_all(outgoing, 'ep', split_axis=0, concat_axis=0, tiled=True)  74.9 us
    all_to_all x1, waiting for transfers between devices, sum_by_parts_2(): jax.lax.all_to_all(jnp.stack(jax.lax.axis_size(across) * [m], axis=0), ax...  58.6 us
    reduce_scatter x2, waiting for transfers between devices, sum_in_order(): pieces = lax.psum_scatter(pieces, axes[k], scatter_dimension=0, tiled=True)  57.2 us
    all_gather x1, waiting for transfers between devices, gather_in_order(): pieces = lax.all_gather(pieces, axes[k], axis=0, tiled=True)  42.1 us
    unnamed x1, blocking collectives  36.2 us
    all_to_all x1, starting transfers between devices, expert_part(): lax.all_to_all(outgoing, 'ep', split_axis=0, concat_axis=0, tiled=True)  13.7 us
    all_to_all x1, starting transfers between devices, sum_by_parts_2(): jax.lax.all_to_all(jnp.stack(jax.lax.axis_size(across) * [m], axis=0), ax...  9.99 us
    all_to_all x1, starting transfers between devices, expert_part(): lax.all_to_all(summed, 'ep', split_axis=0, concat_axis=0, tiled=True)  8.03 us
  transfers between devices with their start and end apart: 9, of which 6 were waited for; matrix products, arithmetic and copies ran while one was open for 20% of the time, Pallas kernels for 0%

profile of v1, /device:TPU:2, one launch (start us, length us, event | category | flops | bytes accessed | tf_op | source)
XLA Modules:
  0.0 388.7 jit_solution(8071785335086545068)
XLA Ops:
  7.2 0.0 copy-start
  7.2 0.8 copy.44
  8.0 0.1 eq.42
  8.1 0.1 eq.38
  8.3 1.2 reduce-window.6
  9.4 0.2 slice_reduce_fusion
  9.7 0.1 fusion.62
  9.8 0.1 reduce_sum.60
  9.9 0.1 copy.47
  10.0 0.7 multiply_add_fusion
  10.7 0.2 fusion.11
  10.9 1.2 fusion.29
  12.1 2.0 convolution_convert_fusion.1
  14.1 2.5 reshape.282
  16.7 0.0 copy-start.5
  16.7 0.0 copy-start.9
  16.7 0.0 copy-start.12
  16.7 0.0 copy-start.10
  16.7 13.7 %all-to-all-start = ((bf16[32,21,2048]{2,1,0:T(8,128)(2,1)}), bf16[32,21,2048]{2,1,0:T(8,128)(2,1)}, u32[]{:S(2)}, u32[]{:S(2)}) async-start(bf16[32,21,2048]{2,1,0:T(8,128)(2,1)} %reshape.282), calls=%async_computation.2 | async-start | bytes 6291456 | tf_op jit(solution)/shard_map/all_to_all | solution.py:184
  30.4 0.0 all-gather.3.cloned.1.call-start
  30.5 0.1 fusion.36
  30.6 0.2 fusion.33
  30.8 0.3 convolution_bitcast_fusion.2
  31.2 0.2 fusion.85
  31.4 0.3 convolution_convert_fusion.4
  31.7 0.3 convolution_convert_fusion.5
  32.0 0.7 pad_maximum_fusion
  32.7 0.0 all-gather.3.cloned.1.call-update
  32.7 74.9 %all-to-all-done = bf16[32,21,2048]{2,1,0:T(8,128)(2,1)} async-done(((bf16[32,21,2048]{2,1,0:T(8,128)(2,1)}), bf16[32,21,2048]{2,1,0:T(8,128)(2,1)}, u32[]{:S(2)}, u32[]{:S(2)}) %all-to-all-start) | async-done | bytes 2752544 | tf_op jit(solution)/shard_map/all_to_all | solution.py:184
  107.6 3.0 reshape.283
  110.6 2.7 convolution_minimum_fusion
  113.3 5.6 %convolution_convert_fusion = bf16[672,2048]{1,0:T(8,128)(2,1)} fusion(bf16[672,2048]{1,0:T(8,128)(2,1)S(1)} %reshape.283, bf16[1,128,2048]{2,1,0:T(8,128)(2,1)S(1)} %copy-done, bf16[1,2048,128]{2,1,0:T(8,128)(2,1)} %param.32, f32[672,128]{1,0:T(8,128)} %convolution_minimum_fusion), kind=kOutput, calls=%fused_computation.11 | convolution fusion | flops 706793472 | bytes 6897664 | tf_op jit(solution)/shard_map/dot_general | solution.py:197
  118.9 36.2 %fusion = bf16[48,2048]{1,0:T(8,128)(2,1)S(1)} fusion(bf16[672,2048]{1,0:T(8,128)(2,1)} %convolution_convert_fusion), kind=kCustom, calls=%all-reduce-scatter | all-reduce-scatter fusion | flops 1572865 | bytes 2951168
  155.1 1.3 collective-permute-start
  156.4 1.3 collective-permute-start.1
  157.8 1.3 dynamic-slice.4
  159.7 2.1 collective-permute-done.1
  161.8 0.8 concatenate.30
  162.6 0.1 constant_dynamic-slice_fusion
  162.6 0.0 copy-start.2
  162.6 2.0 stack.2
  164.7 10.0 %all-to-all-start.1 = ((bf16[16,42,2048]{2,1,0:T(8,128)(2,1)}), bf16[16,42,2048]{2,1,0:T(8,128)(2,1)}, u32[]{:S(2)}, u32[]{:S(2)}) async-start(bf16[16,42,2048]{2,1,0:T(8,128)(2,1)} %stack.2), calls=%async_computation.3 | async-start | bytes 6291456 | tf_op jit(solution)/shard_map/all_to_all | solution.py:66
  174.7 0.0 all-gather.3.cloned.1.call-done
  174.7 6.3 %convolution_bitcast_fusion.1 = f32[1,256,8192]{2,1,0:T(8,128)} fusion(bf16[8192,320]{0,1:T(8,128)(2,1)} %all-gather.3.cloned.1.call-done, bf16[768,128]{1,0:T(8,128)(2,1)S(1)} %copy-done.4, bf16[256,768]{1,0:T(8,128)(2,1)S(1)} %copy-done.2, f32[768]{0:T(1024)S(1)} %copy-done.6, f32[256]{0:T(256)S(1)} %add_rsqrt_fusion.1), kind=kOutput, calls=%fused_computation.1 | convolution fusion | flops 588021760 | bytes 11079680 | tf_op jit(solution)/shard_map/qhd,khd->hqk/dot_general | solution.py:131
  181.0 6.9 %fusion.96 = (f32[256]{0:T(256)S(1)}, f32[1,256,8192]{2,1,0:T(8,128)}) fusion(f32[1,256,8192]{2,1,0:T(8,128)} %convolution_bitcast_fusion.1, bf16[256,32]{0,1:T(8,128)(2,1)S(1)} %get-tuple-element.3, bf16[256,32]{0,1:T(8,128)(2,1)S(1)} %get-tuple-element.2, bf16[8192,320]{0,1:T(8,128)(2,1)} %all-gather.3.cloned.1.call-done, s32[256]{0:T(256)S(1)} %iota_add_fusion), kind=kOutput, calls=%fused_computation.113 | convolution fusion | flops 278986496 | bytes 17860608 | tf_op jit(solution)/shard_map/qhr,kr->hqk/dot_general | solution.py:132
  188.0 58.6 %all-to-all-done.1 = bf16[16,42,2048]{2,1,0:T(8,128)(2,1)} async-done(((bf16[16,42,2048]{2,1,0:T(8,128)(2,1)}), bf16[16,42,2048]{2,1,0:T(8,128)(2,1)}, u32[]{:S(2)}, u32[]{:S(2)}) %all-to-all-start.1) | async-done | bytes 2752544 | tf_op jit(solution)/shard_map/all_to_all | solution.py:66
  246.5 5.3 %reshape.284 = bf16[32,21,2048]{2,1,0:T(8,128)(2,1)} reshape(bf16[16,42,2048]{2,1,0:T(8,128)(2,1)} %all-to-all-done.1) | data formatting | bytes 5505024 | tf_op jit(solution)/shard_map/reshape | solution.py:199
  251.9 8.0 %all-to-all-start.2 = ((bf16[32,21,2048]{2,1,0:T(8,128)(2,1)}), bf16[32,21,2048]{2,1,0:T(8,128)(2,1)}, u32[]{:S(2)}, u32[]{:S(2)}) async-start(bf16[32,21,2048]{2,1,0:T(8,128)(2,1)} %reshape.284), calls=%async_computation.4 | async-start | bytes 6291456 | tf_op jit(solution)/shard_map/all_to_all | solution.py:200
  259.9 0.2 reduce-scatter.5.cloned.1.call-start
  260.2 4.7 %fusion.4 = f32[256]{0:T(256)S(1)} fusion(f32[1,256,8192]{2,1,0:T(8,128)} %get-tuple-element.9, f32[256]{0:T(256)S(1)} %broadcast_maximum_fusion, s32[256]{0:T(256)S(1)} %iota_add_fusion), kind=kLoop, calls=%fused_computation.7 | loop fusion | flops 8388352 | bytes 8391680 | tf_op jit(solution)/shard_map/reduce_sum | solution.py:141
  264.9 7.5 %convolution_convert_fusion.2 = bf16[256,2048]{1,0:T(8,128)(2,1)} fusion(bf16[128,2048]{1,0:T(8,128)(2,1)S(1)} %copy-done.8, bf16[8192,320]{0,1:T(8,128)(2,1)} %all-gather.3.cloned.1.call-done, f32[1,256,8192]{2,1,0:T(8,128)} %get-tuple-element.9, f32[256]{0:T(256)S(1)} %broadcast_maximum_fusion, s32[256]{0:T(256)S(1)} %iota_add_fusion, f32[256]{0:T(256)S(1)} %fusion.4), kind=kOutput, calls=%fused_computation.13 | convolution fusion | flops 680067072 | bytes 12061696 | tf_op jit(solution)/shard_map/dot_general | solution.py:153
  272.3 0.0 reduce-scatter.5.cloned.1.call-update
  272.3 0.0 reduce-scatter.7.cloned.1.call-start
  272.4 39.7 %reduce-scatter.5.cloned.1.call-done = bf16[2,16,2048]{2,1,0:T(8,128)(2,1)} async-done(((bf16[16,16,2048]{2,1,0:T(8,128)(2,1)}), bf16[2,16,2048]{2,1,0:T(8,128)(2,1)}) %reduce-scatter.5.cloned.1.call-update) | async-done | bytes 131088 | tf_op jit(solution)/shard_map/reduce_scatter | solution.py:39
  312.1 0.0 reduce-scatter.7.cloned.1.call-update
  312.1 0.0 all-gather.5.cloned.1.call-start
  312.1 17.5 %reduce-scatter.7.cloned.1.call-done = bf16[1,16,2048]{2,1,0:T(8,128)(2,1)} async-done(((bf16[2,16,2048]{2,1,0:T(8,128)(2,1)}), bf16[1,16,2048]{2,1,0:T(8,128)(2,1)}) %reduce-scatter.7.cloned.1.call-update) | async-done | bytes 65552 | tf_op jit(solution)/shard_map/reduce_scatter | solution.py:39
  329.6 3.6 all_gather.10
  333.2 0.0 all-gather.5.cloned.1.call-update
  333.2 0.1 select_reduce_fusion
  333.4 42.1 %all-gather.5.cloned.1.call-done = bf16[16,16,2048]{2,1,0:T(8,128)(2,1)} async-done(((bf16[2,16,2048]{2,1,0:T(8,128)(2,1)}), bf16[16,16,2048]{2,1,0:T(8,128)(2,1)}) %all-gather.5.cloned.1.call-update) | async-done | bytes 1048592 | tf_op jit(solution)/shard_map/all_gather | solution.py:46
  375.4 3.0 reshape.285
  378.5 1.4 fusion.97
  379.9 2.3 copy.52
  (34 shorter events, 0.2 us)
Async XLA Ops:
  7.2 106.1 %copy-start = (bf16[1,128,2048]{2,1,0:T(8,128)(2,1)S(1)}, bf16[1,128,2048]{2,1,0:T(8,128)(2,1)}, u32[]{:S(2)}) copy-start(bf16[1,128,2048]{2,1,0:T(8,128)(2,1)} %param.33) | copy-start | bytes 1572868
  16.6 13.8 %copy-start.3 = (bf16[256,512]{1,0:T(8,128)(2,1)S(1)}, bf16[256,512]{1,0:T(8,128)(2,1)}, u32[]{:S(2)}) copy-start(bf16[256,512]{1,0:T(8,128)(2,1)} %param.18) | copy-start | bytes 786436
  16.6 13.9 %copy-start.1 = (bf16[256,768]{1,0:T(8,128)(2,1)S(1)}, bf16[256,768]{1,0:T(8,128)(2,1)}, u32[]{:S(2)}) copy-start(bf16[256,768]{1,0:T(8,128)(2,1)} %param.17) | copy-start | bytes 1179652
  16.6 14.1 %copy-start.6 = (f32[768]{0:T(1024)S(1)}, f32[768]{0:T(1024)}, u32[]{:S(2)}) copy-start(f32[768]{0:T(1024)} %param.20) | copy-start | bytes 9220
  16.7 14.1 %copy-start.11 = (bf16[768,64]{0,1:T(8,128)(2,1)S(1)}, bf16[768,64]{0,1:T(8,128)(2,1)}, u32[]{:S(2)}) copy-start(bf16[768,64]{0,1:T(8,128)(2,1)} %param.23) | copy-start | bytes 294916
  16.7 14.5 %copy-start.5 = (bf16[256,64]{0,1:T(8,128)(2,1)S(1)}, bf16[256,64]{0,1:T(8,128)(2,1)}, u32[]{:S(2)}) copy-start(bf16[256,64]{0,1:T(8,128)(2,1)} %param.19) | copy-start | bytes 98308
  16.7 14.7 %copy-start.9 = (bf16[512,128]{1,0:T(8,128)(2,1)S(1)}, bf16[512,128]{1,0:T(8,128)(2,1)}, u32[]{:S(2)}) copy-start(bf16[512,128]{1,0:T(8,128)(2,1)} %param.25) | copy-start | bytes 393220
  16.7 14.7 %copy-start.12 = (f32[512]{0:T(512)S(1)}, f32[512]{0:T(512)}, u32[]{:S(2)}) copy-start(f32[512]{0:T(512)} %param.21) | copy-start | bytes 6148
  16.7 15.0 %copy-start.10 = (bf16[512,128]{1,0:T(8,128)(2,1)S(1)}, bf16[512,128]{1,0:T(8,128)(2,1)}, u32[]{:S(2)}) copy-start(bf16[512,128]{1,0:T(8,128)(2,1)} %param.24) | copy-start | bytes 393220
  16.7 90.9 %all-to-all-start = ((bf16[32,21,2048]{2,1,0:T(8,128)(2,1)}), bf16[32,21,2048]{2,1,0:T(8,128)(2,1)}, u32[]{:S(2)}, u32[]{:S(2)}) async-start(bf16[32,21,2048]{2,1,0:T(8,128)(2,1)} %reshape.282), calls=%async_computation.2 | async-start | bytes 6291456 | tf_op jit(solution)/shard_map/all_to_all | solution.py:184
  30.4 144.3 %all-gather.3.cloned.1.call-start = ((), (), s32[]{:S(2)}) async-start(), calls=%async_computation.5 | async-start | bytes 5406720 | tf_op jit(solution)/shard_map/all_gather | solution.py:21
  155.1 6.7 %collective-permute-start = (bf16[48,2048]{1,0:T(8,128)(2,1)S(1)}, bf16[48,2048]{1,0:T(8,128)(2,1)S(1)}, u32[]{:S(2)}, u32[]{:S(2)}) collective-permute-start(bf16[48,2048]{1,0:T(8,128)(2,1)S(1)} %fusion), channel_id=1, source_target_pairs={{0,1},{1,2},{2,3},{3,4},{4,5},{5,6},{6,7},{7,8},{8,9},{9,10},{10,1... | collective-permute-start | bytes 589832
  156.4 5.3 %collective-permute-start.1 = (bf16[42,2048]{1,0:T(8,128)(2,1)S(1)}, bf16[42,2048]{1,0:T(8,128)(2,1)S(1)}, u32[]{:S(2)}, u32[]{:S(2)}) collective-permute-start(bf16[42,2048]{1,0:T(8,128)(2,1)S(1)} %slice.44), channel_id=1, source_target_pairs={{0,2},{1,3},{2,4},{3,5},{4,6},{5,7},{6,8},{7,9},{8,10},{9,11},{10,... | collective-permute-start | bytes 516104
  162.6 12.1 %copy-start.2 = (bf16[256,768]{1,0:T(8,128)(2,1)S(1)}, bf16[256,768]{1,0:T(8,128)(2,1)}, u32[]{:S(2)}) copy-start(bf16[256,768]{1,0:T(8,128)(2,1)} %param.17) | copy-start | bytes 1179652
  162.6 12.1 %copy-start.4 = (bf16[768,128]{1,0:T(8,128)(2,1)S(1)}, bf16[768,128]{1,0:T(8,128)(2,1)}, u32[]{:S(2)}) copy-start(bf16[768,128]{1,0:T(8,128)(2,1)} %param.22) | copy-start | bytes 589828
  164.7 81.9 %all-to-all-start.1 = ((bf16[16,42,2048]{2,1,0:T(8,128)(2,1)}), bf16[16,42,2048]{2,1,0:T(8,128)(2,1)}, u32[]{:S(2)}, u32[]{:S(2)}) async-start(bf16[16,42,2048]{2,1,0:T(8,128)(2,1)} %stack.2), calls=%async_computation.3 | async-start | bytes 6291456 | tf_op jit(solution)/shard_map/all_to_all | solution.py:66
  251.9 123.5 %all-to-all-start.2 = ((bf16[32,21,2048]{2,1,0:T(8,128)(2,1)}), bf16[32,21,2048]{2,1,0:T(8,128)(2,1)}, u32[]{:S(2)}, u32[]{:S(2)}) async-start(bf16[32,21,2048]{2,1,0:T(8,128)(2,1)} %reshape.284), calls=%async_computation.4 | async-start | bytes 6291456 | tf_op jit(solution)/shard_map/all_to_all | solution.py:200
  259.9 52.1 %reduce-scatter.5.cloned.1.call-start = ((), (), s32[]{:S(2)}) async-start(), calls=%async_computation.6 | async-start | bytes 1179648 | tf_op jit(solution)/shard_map/reduce_scatter | solution.py:39
  260.2 4.7 %copy-start.8 = (bf16[128,2048]{1,0:T(8,128)(2,1)S(1)}, bf16[128,2048]{1,0:T(8,128)(2,1)}, u32[]{:S(2)}) copy-start(bf16[128,2048]{1,0:T(8,128)(2,1)} %param.26) | copy-start | bytes 1572868
  264.8 68.4 %copy-start.7 = (f32[128,4]{0,1:T(4,128)S(1)}, f32[128,4]{0,1:T(4,128)}, u32[]{:S(2)}) copy-start(f32[128,4]{0,1:T(4,128)} %param.30) | copy-start | bytes 6148
  272.3 57.3 %reduce-scatter.7.cloned.1.call-start = ((), (), s32[]{:S(2)}) async-start(), calls=%async_computation.7 | async-start | bytes 196608 | tf_op jit(solution)/shard_map/reduce_scatter | solution.py:39
  312.1 63.3 %all-gather.5.cloned.1.call-start = ((), (), s32[]{:S(2)}) async-start(), calls=%async_computation.8 | async-start | bytes 1179648 | tf_op jit(solution)/shard_map/all_gather | solution.py:46
Sparse Core Ops, SparseCore 0:
  34.8 121.5 all-gather.2
  272.5 39.5 reduce-scatter.4
  314.8 14.7 reduce-scatter.6
  333.3 42.0 all-gather.4
